TPU v7x, 32 devices: a whole 2x2x4 slice. The times are simulated.
32 devices in a mesh: sp: 4 (over y, x), tp: 8 (over z, core).
Axes of the slice: x: 2, y: 2, z: 4, core: 2. Of those that a mesh axis runs over, the one named last changes fastest.
Arguments:
- queries: bfloat16 [2048, 2048], P('sp', 'tp'), may hold values from -8 to 8
- keys: bfloat16 [2048, 1024], P('sp', 'tp'), may hold values from -8 to 8
- values: bfloat16 [2048, 1024], P('sp', 'tp'), may hold values from -6 to 6
- doc_ids: int32 [2048], P('sp'), may hold values from 0 to 1, never falling along the last dimension, each value on 1 to 1536 neighbouring positions
- sink_logits: float32 [32], P('tp'), may hold values from 3 to 6
- out_weight: bfloat16 [2048, 2048], P('tp'), may hold values from -0.75 to 0.75
- residual: bfloat16 [2048, 2048], P(('sp', 'tp')), may hold values from -6 to 6
- norm_gain: float32 [2048], replicated, may hold values from 0.1 to 1.9
- routes: int32 [2048, 2], P(('sp', 'tp')), may hold values from 0 to 3, all different within a row; in each aligned block of 64 rows (0 to 63, 64 to 127, ...) at most 36 rows name the same one
- route_weights: float32 [2048, 2], P(('sp', 'tp')), may hold values from 0.2 to 1
- gate_weight: bfloat16 [4, 2048, 7168], P('sp', None, 'tp'), may hold values from -0.125 to 0.125
- up_weight: bfloat16 [4, 2048, 7168], P('sp', None, 'tp'), may hold values from -0.125 to 0.125
- down_weight: bfloat16 [4, 7168, 2048], P('sp', 'tp'), may hold values from -0.0625 to 0.0625
Outputs:
- layer_output: bfloat16 [2048, 2048], P(('sp', 'tp'))
Inputs may be any that keep to these rules, and one draw needn't show every extreme that they name: `doc_ids`: never falling along the sequence; each document spans 1 to 1536 positions, one exactly that many. `routes`: each row names 2 different experts. In the rows of one device (aligned blocks of 64 rows) no expert is named by more than 36 rows, a bound that some block reaches.
All inputs are finite; a program needn't handle non-finite values.
Results may differ from a plain program's by a relative error of at most 0.015.
Values may be sent and summed in bfloat16 or wider, within the bound.
A program may use at most 128 MiB of HBM per device.

v0:
```python
import math

import jax
import jax.numpy as jnp
from jax import lax
from jax.sharding import PartitionSpec as P

HEAD_DIM = 64
WINDOW = 128


layer_epsilon = 1e-05
masked_score = -1e30


def passed_along(value, axis, steps):
    count = lax.axis_size(axis)
    first, last = (max(0, -steps), min(count, count - steps))
    return lax.ppermute(value, axis, [(source, source + steps) for source in range(first, last)])


def local(
    queries,
    keys,
    values,
    doc_ids,
    sink_logits,
    out_weight,
    residual,
    norm_gain,
    routes,
    route_weights,
    gate_weight,
    up_weight,
    down_weight,
):
    span_rows = queries.shape[0]
    kv_width = keys.shape[1]
    kv_groups = kv_width // HEAD_DIM
    heads_here = queries.shape[1] // HEAD_DIM
    group_ratio = heads_here // kv_groups
    reach_back = WINDOW - 1
    score_scale = 1.0 / math.sqrt(HEAD_DIM)
    doc_float = (doc_ids + 1).astype(jnp.float32)
    key_value = jnp.concatenate([keys, values], axis=1).astype(jnp.float32)
    tail_pairs, tail_docs = (
        passed_along(key_value[span_rows - reach_back :].astype(jnp.bfloat16), "sp", 1).astype(
            jnp.float32
        ),
        passed_along(doc_float[span_rows - reach_back :].astype(jnp.bfloat16), "sp", 1).astype(
            jnp.float32
        ),
    )
    all_keys = jnp.concatenate([tail_pairs[:, :kv_width].astype(jnp.bfloat16), keys], axis=0)
    all_values = jnp.concatenate([tail_pairs[:, kv_width:].astype(jnp.bfloat16), values], axis=0)
    all_docs = jnp.concatenate([tail_docs, doc_float], axis=0)
    block_rows = min(512, span_rows)
    sink_table = sink_logits.reshape(kv_groups, group_ratio, 1)
    offsets = (
        jnp.arange(block_rows)[:, None] + reach_back - jnp.arange(block_rows + reach_back)[None, :]
    )
    window_mask = (offsets >= 0) & (offsets <= reach_back)
    pieces = []
    for block_index in range(span_rows // block_rows):
        first_row = block_index * block_rows
        query_rows = queries[first_row : first_row + block_rows].reshape(
            block_rows, kv_groups, group_ratio, HEAD_DIM
        )
        key_rows = all_keys[first_row : first_row + block_rows + reach_back].reshape(
            block_rows + reach_back, kv_groups, HEAD_DIM
        )
        value_rows = all_values[first_row : first_row + block_rows + reach_back].reshape(
            block_rows + reach_back, kv_groups, HEAD_DIM
        )
        scores = (
            jnp.einsum("bgrd,sgd->grbs", query_rows, key_rows, preferred_element_type=jnp.float32)
            * score_scale
        )
        same_doc = (
            doc_float[first_row : first_row + block_rows][:, None]
            == all_docs[first_row : first_row + block_rows + reach_back][None, :]
        )
        scores = jnp.where(window_mask & same_doc, scores, masked_score)
        row_max = jnp.maximum(scores.max(-1), sink_table)
        exp_scores = jnp.exp(scores - row_max[..., None])
        denominator = exp_scores.sum(-1) + jnp.exp(sink_table - row_max)
        weighted = jnp.einsum(
            "grbs,sgd->bgrd",
            exp_scores.astype(jnp.bfloat16),
            value_rows,
            preferred_element_type=jnp.float32,
        )
        weighted = weighted / jnp.transpose(denominator, (2, 0, 1))[..., None]
        pieces.append(weighted.astype(jnp.bfloat16).reshape(block_rows, heads_here * HEAD_DIM))
    attended = jnp.concatenate(pieces, axis=0)
    rows_here = attended
    projected = lax.psum_scatter(
        jnp.dot(rows_here, out_weight, preferred_element_type=jnp.float32).astype(jnp.bfloat16),
        "tp",
        scatter_dimension=0,
        tiled=True,
    ).astype(jnp.float32)
    stream = residual.astype(jnp.float32) + projected
    mean_value = stream.mean(-1, keepdims=True)
    centred = stream - mean_value
    variance = (centred * centred).mean(-1, keepdims=True)
    normed = (centred * lax.rsqrt(variance + layer_epsilon) * norm_gain).astype(jnp.bfloat16)
    token_count = residual.shape[0]
    width = residual.shape[1]
    route_count = routes.shape[1]
    expert_count = lax.axis_size("sp") * gate_weight.shape[0]
    capacity = 9 * route_count * token_count // (8 * expert_count)
    flat_routes = routes.reshape(-1)
    one_hot = (flat_routes[:, None] == jnp.arange(expert_count)[None, :]).astype(jnp.int32)
    slot_ids = jnp.sum((jnp.cumsum(one_hot, axis=0) - 1) * one_hot, axis=1)
    destination = flat_routes * capacity + slot_ids
    slot_range = jnp.arange(expert_count * capacity)
    selector = jnp.any(
        slot_range[:, None, None] == destination.reshape(token_count, route_count)[None], axis=2
    )
    dispatch = jnp.dot(
        selector.astype(jnp.bfloat16), normed, preferred_element_type=jnp.float32
    ).astype(jnp.bfloat16)
    inbound = lax.all_to_all(
        dispatch.reshape(expert_count, capacity, width),
        "sp",
        split_axis=0,
        concat_axis=0,
        tiled=True,
    )
    arrived = inbound.reshape(-1, width)
    row_piece = lax.all_gather(arrived, "tp", axis=0, tiled=True)
    gate = jnp.dot(row_piece, gate_weight[0], preferred_element_type=jnp.float32)
    upward = jnp.dot(row_piece, up_weight[0], preferred_element_type=jnp.float32)
    hidden = (jax.nn.silu(gate) * upward).astype(jnp.bfloat16)
    rows_here = hidden
    partial_value = jnp.dot(rows_here, down_weight[0], preferred_element_type=jnp.float32).astype(
        jnp.bfloat16
    )
    returned = lax.psum_scatter(
        lax.optimization_barrier(partial_value).astype(jnp.float32).astype(jnp.bfloat16),
        "tp",
        scatter_dimension=0,
        tiled=True,
    )
    back_rows = lax.all_to_all(
        returned.reshape(inbound.shape), "sp", split_axis=0, concat_axis=0, tiled=True
    ).reshape(-1, width)
    picked = back_rows[destination].astype(jnp.float32).reshape(token_count, route_count, width)
    combined = jnp.sum(picked * route_weights[..., None], axis=1)
    return (stream + combined).astype(jnp.bfloat16)


def solution(mesh):
    placed = (
        P("sp", "tp"),
        P("sp", "tp"),
        P("sp", "tp"),
        P("sp"),
        P("tp"),
        P("tp", None),
        P(("sp", "tp"), None),
        P(),
        P(("sp", "tp"), None),
        P(("sp", "tp"), None),
        P("sp", None, "tp"),
        P("sp", None, "tp"),
        P("sp", "tp", None),
    )
    return jax.shard_map(
        local, mesh=mesh, in_specs=placed, out_specs=P(("sp", "tp"), None), check_vma=False
    )
```

profile of v0, /device:TPU:8, one launch (start us, length us, event | category | flops | bytes accessed | tf_op | source)
XLA Modules:
  0.0 231.3 jit_solution(13959658188333084272)
XLA Ops:
  7.4 3.4 %collective-permute-start.1 = (bf16[127]{0:T(256)(128)(2,1)S(1)}, bf16[127]{0:T(256)(128)(2,1)S(1)}, u32[]{:S(2)}, u32[]{:S(2)}) collective-permute-start(bf16[127]{0:T(256)(128)(2,1)S(1)} %slice.18), channel_id=1, source_target_pairs={{0,8},{8,16},{16,24},{1,9},{9,17},{17,25},{2,10},{10,18},{18,26},{... | collective-permute-start | bytes 770 | tf_op jit(solution)/shard_map/ppermute | solution.py:19
  11.6 3.4 %collective-permute-start = (bf16[127,256]{1,0:T(8,128)(2,1)S(1)}, bf16[127,256]{1,0:T(8,128)(2,1)S(1)}, u32[]{:S(2)}, u32[]{:S(2)}) collective-permute-start(bf16[127,256]{1,0:T(8,128)(2,1)S(1)} %pad_maximum_fusion.2), channel_id=1, source_target_pairs={{0,8},{8,16},{16,24},{1,9},{9,17},{17,25},{2,10},{10,18},{18,26},{... | collective-permute-start | bytes 195080 | tf_op jit(solution)/shard_map/ppermute | solution.py:19
  15.0 1.1 copy.30
  17.4 1.0 pad_maximum_fusion
  18.6 1.1 fusion.2
  19.8 2.2 copy-done.1
  22.0 1.1 fusion
  23.4 4.0 %fusion.23 = bf16[512,2,2,64]{0,3,2,1:T(8,128)(2,1)S(1)} fusion(bf16[639,2,64,1]{0,2,3,1:T(8,128)(2,1)S(1)} %bitcast.63, f32[2,639,512,2]{2,1,3,0:T(8,128)} %copy-done.1, f32[2,2,512]{2,1,0:T(2,128)S(1)} %broadcast_maximum_fusion, pred[512,639]{0,1:T(8,128)(4,1)S(1)} %fusion.16, f32[512,2,2]{0,2,1:T(2,128)S(1)} %add_bitcast_fusion), kind=kOutput, calls=%fused_computation.25 | convolution fusion | flops 173006848 | bytes 6003968 | tf_op jit(solution)/shard_map/grbs,sgd->bgrd/dot_general | solution.py:87
  27.4 2.1 convolution_convert_fusion.1
  30.6 32.8 %reduce-scatter.3.cloned.1.call-done = bf16[64,2048]{1,0:T(8,128)(2,1)} async-done(((bf16[512,2048]{1,0:T(8,128)(2,1)}), bf16[64,2048]{1,0:T(8,128)(2,1)}) %reduce-scatter.3.cloned.1.call-update) | async-done | bytes 262160 | tf_op jit(solution)/shard_map/reduce_scatter | solution.py:97
  63.5 1.1 fusion.26
  64.6 1.2 multiply_reduce_fusion.1
  65.8 1.3 convolution_convert_fusion.2
  67.3 11.9 %all_to_all.10 = bf16[4,36,2048]{2,1,0:T(8,128)(2,1)S(1)} all-to-all(bf16[4,36,2048]{2,1,0:T(8,128)(2,1)S(1)} %reshape.95), channel_id=1, replica_groups=mesh['sp'=4,'tp'=8] {'sp'}, dimensions={0} | all-to-all | bytes 1179648 | tf_op jit(solution)/shard_map/all_to_all | solution.py:124
  79.1 1.0 reshape.96
  80.4 51.3 %all-gather.2.cloned.1.call-done = bf16[1152,2048]{1,0:T(8,128)(2,1)} async-done(((bf16[144,2048]{1,0:T(8,128)(2,1)}), bf16[1152,2048]{1,0:T(8,128)(2,1)}) %all-gather.2.cloned.1.call-update) | async-done | bytes 4718608 | tf_op jit(solution)/shard_map/all_gather | solution.py:132
  131.7 8.1 %fusion.5 = f32[1152,896]{1,0:T(8,128)S(1)} fusion(bf16[1152,2048]{1,0:T(8,128)(2,1)} %all-gather.2.cloned.1.call-done, bf16[1,2048,896]{2,1,0:T(8,128)(2,1)} %param.23), kind=kOutput, calls=%fused_computation.10 | convolution fusion | flops 4227858432 | bytes 12517376 | tf_op jit(solution)/shard_map/dot_general | solution.py:133
  139.8 5.3 %fusion.7 = bf16[1152,896]{1,0:T(8,128)(2,1)S(1)} fusion(bf16[1152,2048]{1,0:T(8,128)(2,1)S(1)} %copy-done.7, bf16[1,2048,896]{2,1,0:T(8,128)(2,1)S(1)} %copy-done.8, f32[1152,896]{1,0:T(8,128)S(1)} %fusion.5), kind=kOutput, calls=%fused_computation.12 | convolution fusion | flops 4234051584 | bytes 14581760 | tf_op jit(solution)/shard_map/dot_general | solution.py:134
  145.2 6.7 %convolution_convert_fusion = bf16[1152,2048]{1,0:T(8,128)(2,1)} fusion(bf16[1152,896]{1,0:T(8,128)(2,1)S(1)} %fusion.7, bf16[1,896,2048]{2,1,0:T(8,128)(2,1)S(1)} %copy-done.9), kind=kOutput, calls=%fused_computation.1 | convolution fusion | flops 4230217728 | bytes 10452992 | tf_op jit(solution)/shard_map/dot_general | solution.py:137
  151.9 52.2 %reduce-scatter.5.cloned.1.call-done = bf16[144,2048]{1,0:T(8,128)(2,1)} async-done(((bf16[1152,2048]{1,0:T(8,128)(2,1)}), bf16[144,2048]{1,0:T(8,128)(2,1)}) %reduce-scatter.5.cloned.1.call-update) | async-done | bytes 589840 | tf_op jit(solution)/shard_map/reduce_scatter | solution.py:140
  204.1 2.0 reshape.97
  206.1 3.9 %all-to-all-start.1 = ((bf16[4,36,2048]{2,1,0:T(8,128)(2,1)}), bf16[4,36,2048]{2,1,0:T(8,128)(2,1)S(1)}, u32[]{:S(2)}, u32[]{:S(2)}) async-start(bf16[4,36,2048]{2,1,0:T(8,128)(2,1)} %reshape.97), calls=%async_computation.3 | async-start | bytes 1310720 | tf_op jit(solution)/shard_map/all_to_all | solution.py:146
  210.3 10.4 %all-to-all-done.1 = bf16[4,36,2048]{2,1,0:T(8,128)(2,1)S(1)} async-done(((bf16[4,36,2048]{2,1,0:T(8,128)(2,1)}), bf16[4,36,2048]{2,1,0:T(8,128)(2,1)S(1)}, u32[]{:S(2)}, u32[]{:S(2)}) %all-to-all-start.1) | async-done | bytes 589856 | tf_op jit(solution)/shard_map/all_to_all | solution.py:146
  222.4 1.5 multiply_reduce_fusion
  (60 shorter events, 7.6 us)
Async XLA Ops:
  6.5 20.9 %copy-start = (bf16[256,2048]{1,0:T(8,128)(2,1)S(1)}, bf16[256,2048]{1,0:T(8,128)(2,1)}, u32[]{:S(2)}) copy-start(bf16[256,2048]{1,0:T(8,128)(2,1)} %param.18) | copy-start | bytes 3145732
  6.5 56.9 %reduce-scatter.3.cloned.1.call-start = ((), (), s32[]{:S(2)}) async-start(), calls=%async_computation.4 | async-start | bytes 2359296 | tf_op jit(solution)/shard_map/reduce_scatter | solution.py:97
  7.4 9.5 %collective-permute-start.1 = (bf16[127]{0:T(256)(128)(2,1)S(1)}, bf16[127]{0:T(256)(128)(2,1)S(1)}, u32[]{:S(2)}, u32[]{:S(2)}) collective-permute-start(bf16[127]{0:T(256)(128)(2,1)S(1)} %slice.18), channel_id=1, source_target_pairs={{0,8},{8,16},{16,24},{1,9},{9,17},{17,25},{2,10},{10,18},{18,26},{... | collective-permute-start | bytes 770 | tf_op jit(solution)/shard_map/ppermute | solution.py:19
  11.6 5.8 %collective-permute-start = (bf16[127,256]{1,0:T(8,128)(2,1)S(1)}, bf16[127,256]{1,0:T(8,128)(2,1)S(1)}, u32[]{:S(2)}, u32[]{:S(2)}) collective-permute-start(bf16[127,256]{1,0:T(8,128)(2,1)S(1)} %pad_maximum_fusion.2), channel_id=1, source_target_pairs={{0,8},{8,16},{16,24},{1,9},{9,17},{17,25},{2,10},{10,18},{18,26},{... | collective-permute-start | bytes 195080 | tf_op jit(solution)/shard_map/ppermute | solution.py:19
  19.7 2.3 copy-start.1
  27.4 2.2 copy-start.5
  27.4 36.1 %copy-start.2 = (bf16[64,2048]{1,0:T(8,128)(2,1)S(1)}, bf16[64,2048]{1,0:T(8,128)(2,1)}, u32[]{:S(2)}) copy-start(bf16[64,2048]{1,0:T(8,128)(2,1)} %param.19) | copy-start | bytes 786436
  27.4 38.4 %copy-start.4 = (f32[2048]{0:T(1024)S(1)}, f32[2048]{0:T(1024)}, u32[]{:S(2)}) copy-start(f32[2048]{0:T(1024)} %param.20) | copy-start | bytes 24580
  29.6 102.1 %all-gather.2.cloned.1.call-start = ((), (), s32[]{:S(2)}) async-start(), calls=%async_computation.5 | async-start | bytes 5308416 | tf_op jit(solution)/shard_map/all_gather | solution.py:132
  80.1 124.0 %reduce-scatter.5.cloned.1.call-start = ((), (), s32[]{:S(2)}) async-start(), calls=%async_computation.6 | async-start | bytes 5308416 | tf_op jit(solution)/shard_map/reduce_scatter | solution.py:140
  131.7 8.1 %copy-start.7 = (bf16[1152,2048]{1,0:T(8,128)(2,1)S(1)}, bf16[1152,2048]{1,0:T(8,128)(2,1)}, u32[]{:S(2)}) copy-start(bf16[1152,2048]{1,0:T(8,128)(2,1)} %all-gather.2.cloned.1.call-done) | copy-start | bytes 14155780
  131.7 8.1 %copy-start.8 = (bf16[1,2048,896]{2,1,0:T(8,128)(2,1)S(1)}, bf16[1,2048,896]{2,1,0:T(8,128)(2,1)}, u32[]{:S(2)}) copy-start(bf16[1,2048,896]{2,1,0:T(8,128)(2,1)} %param.24) | copy-start | bytes 11010052
  139.8 5.3 %copy-start.9 = (bf16[1,896,2048]{2,1,0:T(8,128)(2,1)S(1)}, bf16[1,896,2048]{2,1,0:T(8,128)(2,1)}, u32[]{:S(2)}) copy-start(bf16[1,896,2048]{2,1,0:T(8,128)(2,1)} %param.25) | copy-start | bytes 11010052
  151.9 58.3 %copy-start.6 = (f32[64,2]{0,1:T(2,128)S(1)}, f32[64,2]{0,1:T(2,128)}, u32[]{:S(2)}) copy-start(f32[64,2]{0,1:T(2,128)} %param.22) | copy-start | bytes 1540
  206.1 14.5 %all-to-all-start.1 = ((bf16[4,36,2048]{2,1,0:T(8,128)(2,1)}), bf16[4,36,2048]{2,1,0:T(8,128)(2,1)S(1)}, u32[]{:S(2)}, u32[]{:S(2)}) async-start(bf16[4,36,2048]{2,1,0:T(8,128)(2,1)} %reshape.97), calls=%async_computation.3 | async-start | bytes 1310720 | tf_op jit(solution)/shard_map/all_to_all | solution.py:146
  220.8 3.2 %copy-start.3 = (bf16[64,2048]{1,0:T(8,128)(2,1)S(1)}, bf16[64,2048]{1,0:T(8,128)(2,1)}, u32[]{:S(2)}) copy-start(bf16[64,2048]{1,0:T(8,128)(2,1)} %reduce-scatter.3.cloned.1.call-done) | copy-start | bytes 786436
Sparse Core Ops, SparseCore 0:
  29.7 33.7 reduce-scatter.2
  80.2 51.3 all-gather.1
  152.0 52.0 reduce-scatter.4
where the time goes:
time: 233 us; the launch traced here: 231 us
  waiting for transfers between devices  147 us (63%)
  matrix products  28.7 us (12%)
  between operations  13.4 us (6%)
  blocking collectives  11.9 us (5%)
  starting transfers between devices  11 us (5%)
  local copies, waits for them, and re-layouts  9.97 us (4%)
  other arithmetic  9.64 us (4%)
    reduce_scatter x1, waiting for transfers between devices, local(): lax.psum_scatter(lax.optimization_barrier(partial_value).astype(jnp.float...  52.2 us
    all_gather x1, waiting for transfers between devices, local(): row_piece = lax.all_gather(arrived, 'tp', axis=0, tiled=True)  51.3 us
    reduce_scatter x1, waiting for transfers between devices, local(): lax.psum_scatter(jnp.dot(rows_here, out_weight, preferred_element_type=jn...  32.8 us
    all_to_all x1, blocking collectives, local(): lax.all_to_all(dispatch.reshape(expert_count, capacity, width), 'sp', spl...  11.9 us
    all_to_all x1, waiting for transfers between devices, local(): lax.all_to_all(returned.reshape(inbound.shape), 'sp', split_axis=0, conca...  10.4 us
    dot_general x1, matrix products, local(): jnp.dot(row_piece, gate_weight[0], preferred_element_type=jnp.float32)  8.11 us
    ppermute x2, starting transfers between devices, passed_along(): lax.ppermute(value, axis, [(source, source + steps) for source in range(f...  6.79 us
    dot_general x1, matrix products, local(): jnp.dot(rows_here, down_weight[0], preferred_element_type=jnp.float32)  6.72 us
  transfers between devices with their start and end apart: 6, of which 4 were waited for; matrix products, arithmetic and copies ran while one was open for 2% of the time, Pallas kernels for 0%

commit v1 on v0

--- a/solution.py
+++ b/solution.py
@@ -1,8 +1,11 @@
+import functools
 import math
 
 import jax
 import jax.numpy as jnp
 from jax import lax
+from jax.experimental import pallas as pl
+from jax.experimental.pallas import tpu as pltpu
 from jax.sharding import PartitionSpec as P
 
 HEAD_DIM = 64
@@ -17,6 +20,447 @@
     count = lax.axis_size(axis)
     first, last = (max(0, -steps), min(count, count - steps))
     return lax.ppermute(value, axis, [(source, source + steps) for source in range(first, last)])
+
+
+VMEM = pl.BlockSpec(memory_space=pltpu.VMEM)
+
+
+def remote(source, target, sent, landed, device):
+    return pltpu.make_async_remote_copy(
+        src_ref=source,
+        dst_ref=target,
+        send_sem=sent,
+        recv_sem=landed,
+        device_id=device,
+        device_id_type=pl.DeviceIdType.MESH,
+    )
+
+
+def tp_place():
+    me = lax.axis_index("tp")
+    chip, core = me // 2, lax.rem(me, 2)
+    return chip, core, chip * 2 + 1 - core, me - 2, me + 2
+
+
+def greet(chips, spans):
+    chip, _, partner, before, after = tp_place()
+    span = lax.axis_index("sp")
+    barrier = pltpu.get_barrier_semaphore()
+
+    def hello(device):
+        pl.semaphore_signal(
+            barrier, inc=1, device_id=device, device_id_type=pl.DeviceIdType.MESH
+        )
+
+    hello({"tp": partner})
+    pl.when(chip > 0)(lambda: hello({"tp": before}))
+    pl.when(chip < chips - 1)(lambda: hello({"tp": after}))
+    for step in range(1, spans):
+        hello({"sp": lax.rem(span + step, spans)})
+    inner = jnp.where(chip > 0, 1, 0) + jnp.where(chip < chips - 1, 1, 0)
+    pl.semaphore_wait(barrier, inner + spans)
+
+
+def outside_in(count):
+    order = []
+    for step in range((count + 1) // 2):
+        order.extend([count - 1 - step] + ([step] if step != count - 1 - step else []))
+    return order
+
+
+def column_loop(width, body):
+    step = min(512, width)
+
+    def one(index, carry):
+        body(pl.ds(pl.multiple_of(index * step, step), step))
+        return carry
+
+    lax.fori_loop(0, width // step, one, 0)
+
+
+def line_step(chips, block, term, width, total, travel, held, sent, landed):
+    chip, _, _, before, after = tp_place()
+    for way, passes, receives, device in (
+        (0, chip < block, chip > 0, {"tp": after}),
+        (1, chip > block, chip < chips - 1, {"tp": before}),
+    ):
+        copy = remote(
+            travel.at[block], held.at[way, block], sent.at[block], landed.at[way, block], device
+        )
+
+        @pl.when(passes & receives)
+        def _(copy=copy, way=way):
+            copy.wait_recv()
+
+            def add(columns):
+                travel[block, :, columns] = (
+                    term(columns) + held[way, block, :, columns].astype(jnp.float32)
+                ).astype(jnp.bfloat16)
+
+            column_loop(width, add)
+
+        @pl.when(passes & jnp.logical_not(receives))
+        def _():
+            def keep(columns):
+                travel[block, :, columns] = term(columns).astype(jnp.bfloat16)
+
+            column_loop(width, keep)
+
+        pl.when(passes)(copy.start)
+
+    @pl.when(chip == block)
+    def _():
+        def keep(columns):
+            total[:, columns] = term(columns)
+
+        column_loop(width, keep)
+
+
+def line_finish(chips, width, total, travel, held, sent, landed):
+    chip, _, _, before, after = tp_place()
+    for way, receives in ((0, chip > 0), (1, chip < chips - 1)):
+
+        @pl.when(receives)
+        def _(way=way):
+            remote(
+                travel.at[chip],
+                held.at[way, chip],
+                sent.at[chip],
+                landed.at[way, chip],
+                {"tp": after},
+            ).wait_recv()
+
+            def add(columns):
+                total[:, columns] = total[:, columns] + held[way, chip, :, columns].astype(
+                    jnp.float32
+                )
+
+            column_loop(width, add)
+
+    for block in range(chips):
+        copy = remote(
+            travel.at[block], held.at[0, block], sent.at[block], landed.at[0, block], {"tp": after}
+        )
+        pl.when(chip != block)(copy.wait_send)
+
+
+def sum_kernel(
+    chips, parts, total, arrived, travel, held, core_sent, core_landed, sent, landed
+):
+    _, core, partner, _, _ = tp_place()
+    width = parts.shape[-1]
+    greet(chips, 1)
+
+    def handed(block):
+        return remote(
+            parts.at[block, 1 - core],
+            arrived.at[block],
+            core_sent.at[block],
+            core_landed.at[block],
+            {"tp": partner},
+        )
+
+    for block in outside_in(chips):
+        handed(block).start()
+    for block in outside_in(chips):
+        handed(block).wait_recv()
+
+        def term(columns, block=block):
+            return parts[block, core, :, columns].astype(jnp.float32) + arrived[
+                block, :, columns
+            ].astype(jnp.float32)
+
+        line_step(chips, block, term, width, total, travel, held, sent, landed)
+    line_finish(chips, width, total, travel, held, sent, landed)
+    for block in range(chips):
+        handed(block).wait_send()
+
+
+def tp_sum(parts):
+    chips, _, rows, width = parts.shape
+    dma = pltpu.SemaphoreType.DMA
+    return pl.pallas_call(
+        functools.partial(sum_kernel, chips),
+        out_shape=jax.ShapeDtypeStruct((rows, width), jnp.float32),
+        in_specs=[VMEM],
+        out_specs=VMEM,
+        scratch_shapes=[
+            pltpu.VMEM((chips, rows, width), jnp.bfloat16),
+            pltpu.VMEM((chips, rows, width), jnp.bfloat16),
+            pltpu.VMEM((2, chips, rows, width), jnp.bfloat16),
+            dma((chips,)),
+            dma((chips,)),
+            dma((chips,)),
+            dma((2, chips)),
+        ],
+        compiler_params=pltpu.CompilerParams(
+            collective_id=0, has_side_effects=True, vmem_limit_bytes=60 << 20
+        ),
+    )(parts)
+
+
+def spread_kernel(
+    chips,
+    spans,
+    picks,
+    normed,
+    notes,
+    rows,
+    all_notes,
+    blocks,
+    outgoing,
+    line_sent,
+    line_landed,
+    note_sent,
+    note_landed,
+    span_sent,
+    span_landed,
+    core_sent,
+    core_landed,
+):
+    chip, core, partner, before, after = tp_place()
+    span = lax.axis_index("sp")
+    count, width = normed.shape
+    slots = rows.shape[3]
+    greet(chips, spans)
+    all_notes[chip] = notes[...]
+
+    def pass_on(block, way, first):
+        device = {"tp": after if way == 0 else before}
+        return (
+            remote(
+                normed if first else blocks.at[block],
+                blocks.at[block],
+                line_sent.at[way, block],
+                line_landed.at[block],
+                device,
+            ),
+            remote(
+                notes if first else all_notes.at[block],
+                all_notes.at[block],
+                note_sent.at[way, block],
+                note_landed.at[block],
+                device,
+            ),
+        )
+
+    def to_span(block, step):
+        other = lax.rem(span + step, spans)
+        return remote(
+            outgoing.at[block, other],
+            rows.at[core, block, span],
+            span_sent.at[block, step],
+            span_landed.at[block, step],
+            {"sp": other},
+        )
+
+    def to_partner(block):
+        return remote(
+            rows.at[core, block],
+            rows.at[core, block],
+            core_sent.at[block],
+            core_landed.at[block],
+            {"tp": partner},
+        )
+
+    def hand_out(block, source, note):
+        listing = note[...][:picks, :count]
+        for expert in range(spans):
+            slot = (
+                lax.broadcasted_iota(jnp.int32, (slots, count), 0) + expert * slots
+            ).astype(jnp.float32)
+            chosen = jnp.zeros((slots, count), jnp.float32)
+            for pick in range(picks):
+                chosen = jnp.where(slot == listing[pick : pick + 1], 1.0, chosen)
+            chosen = chosen.astype(jnp.bfloat16)
+
+            def select(columns, expert=expert, chosen=chosen):
+                outgoing[block, expert, :, columns] = jnp.dot(
+                    chosen, source[:, columns], preferred_element_type=jnp.float32
+                ).astype(jnp.bfloat16)
+
+            column_loop(width, select)
+        for step in range(1, spans):
+            to_span(block, step).start()
+        rows[core, block, span] = outgoing[block, span]
+
+    def start_both(block, way, first):
+        for copy in pass_on(block, way, first):
+            copy.start()
+
+    pl.when(chip < chips - 1)(lambda: start_both(chip, 0, True))
+    pl.when(chip > 0)(lambda: start_both(chip, 1, True))
+    hand_out(chip, normed, notes)
+    for step in range(1, chips):
+        for way, block, present, further in (
+            (0, chip - step, chip >= step, chip < chips - 1),
+            (1, chip + step, chip + step < chips, chip > 0),
+        ):
+
+            @pl.when(present)
+            def _(way=way, block=block, further=further):
+                for copy in pass_on(block, way, False):
+                    copy.wait_recv()
+                pl.when(further)(lambda: start_both(block, way, False))
+                hand_out(block, blocks.at[block], all_notes.at[block])
+
+    def finish(block):
+        for step in range(1, spans):
+            to_span(block, step).wait_recv()
+        to_partner(block).start()
+
+    finish(chip)
+    for step in range(1, chips):
+        pl.when(chip >= step)(lambda step=step: finish(chip - step))
+        pl.when(chip + step < chips)(lambda step=step: finish(chip + step))
+
+    def wait_both(block, way, first):
+        for copy in pass_on(block, way, first):
+            copy.wait_send()
+
+    for block in range(chips):
+        pl.when((chip >= block) & (chip < chips - 1))(lambda block=block: wait_both(block, 0, False))
+        pl.when((chip <= block) & (chip > 0))(lambda block=block: wait_both(block, 1, False))
+        for step in range(1, spans):
+            to_span(block, step).wait_send()
+        to_partner(block).wait()
+
+
+def spread(normed, notes, chips, spans, slots, picks):
+    count, width = normed.shape
+    dma = pltpu.SemaphoreType.DMA
+    return pl.pallas_call(
+        functools.partial(spread_kernel, chips, spans, picks),
+        out_shape=(
+            jax.ShapeDtypeStruct((2, chips, spans, slots, width), jnp.bfloat16),
+            jax.ShapeDtypeStruct((chips,) + notes.shape, jnp.float32),
+        ),
+        in_specs=[VMEM, VMEM],
+        out_specs=(VMEM, VMEM),
+        scratch_shapes=[
+            pltpu.VMEM((chips, count, width), jnp.bfloat16),
+            pltpu.VMEM((chips, spans, slots, width), jnp.bfloat16),
+            dma((2, chips)),
+            dma((chips,)),
+            dma((2, chips)),
+            dma((chips,)),
+            dma((chips, spans)),
+            dma((chips, spans)),
+            dma((chips,)),
+            dma((chips,)),
+        ],
+        compiler_params=pltpu.CompilerParams(
+            collective_id=1, has_side_effects=True, vmem_limit_bytes=60 << 20
+        ),
+    )(normed, notes)
+
+
+def collect_kernel(
+    chips,
+    spans,
+    parts,
+    shares,
+    total,
+    arrived,
+    outgoing,
+    gathered,
+    travel,
+    held,
+    core_sent,
+    core_landed,
+    span_sent,
+    span_landed,
+    sent,
+    landed,
+):
+    _, core, partner, _, _ = tp_place()
+    span = lax.axis_index("sp")
+    width = parts.shape[-1]
+    greet(chips, spans)
+
+    def handed(block):
+        return remote(
+            parts.at[1 - core, block],
+            arrived.at[block],
+            core_sent.at[block],
+            core_landed.at[block],
+            {"tp": partner},
+        )
+
+    def to_span(block, step):
+        other = lax.rem(span + step, spans)
+        return remote(
+            outgoing.at[block, other],
+            gathered.at[block, span],
+            span_sent.at[block, step],
+            span_landed.at[block, step],
+            {"sp": other},
+        )
+
+    for block in outside_in(chips):
+        handed(block).start()
+    for block in outside_in(chips):
+        handed(block).wait_recv()
+
+        def add(columns, block=block):
+            outgoing[block, :, :, columns] = (
+                parts[core, block, :, :, columns].astype(jnp.float32)
+                + arrived[block, :, :, columns].astype(jnp.float32)
+            ).astype(jnp.bfloat16)
+
+        column_loop(width, add)
+        for step in range(1, spans):
+            to_span(block, step).start()
+        gathered[block, span] = outgoing[block, span]
+    for block in outside_in(chips):
+        for step in range(1, spans):
+            to_span(block, step).wait_recv()
+
+        def term(columns, block=block):
+            result = None
+            for expert in range(spans):
+                share = jnp.dot(
+                    shares[block, expert],
+                    gathered[block, expert, :, columns],
+                    preferred_element_type=jnp.float32,
+                )
+                result = share if result is None else result + share
+            return result
+
+        line_step(chips, block, term, width, total, travel, held, sent, landed)
+    line_finish(chips, width, total, travel, held, sent, landed)
+    for block in range(chips):
+        handed(block).wait_send()
+        for step in range(1, spans):
+            to_span(block, step).wait_send()
+
+
+def collect(parts, shares):
+    _, chips, spans, slots, width = parts.shape
+    rows = shares.shape[2]
+    dma = pltpu.SemaphoreType.DMA
+    return pl.pallas_call(
+        functools.partial(collect_kernel, chips, spans),
+        out_shape=jax.ShapeDtypeStruct((rows, width), jnp.float32),
+        in_specs=[VMEM, VMEM],
+        out_specs=VMEM,
+        scratch_shapes=[
+            pltpu.VMEM((chips, spans, slots, width), jnp.bfloat16),
+            pltpu.VMEM((chips, spans, slots, width), jnp.bfloat16),
+            pltpu.VMEM((chips, spans, slots, width), jnp.bfloat16),
+            pltpu.VMEM((chips, rows, width), jnp.bfloat16),
+            pltpu.VMEM((2, chips, rows, width), jnp.bfloat16),
+            dma((chips,)),
+            dma((chips,)),
+            dma((chips, spans)),
+            dma((chips, spans)),
+            dma((chips,)),
+            dma((2, chips)),
+        ],
+        compiler_params=pltpu.CompilerParams(
+            collective_id=2, has_side_effects=True, vmem_limit_bytes=60 << 20
+        ),
+    )(parts, shares)
 
 
 def local(
@@ -94,60 +538,47 @@
         pieces.append(weighted.astype(jnp.bfloat16).reshape(block_rows, heads_here * HEAD_DIM))
     attended = jnp.concatenate(pieces, axis=0)
     rows_here = attended
-    projected = lax.psum_scatter(
-        jnp.dot(rows_here, out_weight, preferred_element_type=jnp.float32).astype(jnp.bfloat16),
-        "tp",
-        scatter_dimension=0,
-        tiled=True,
-    ).astype(jnp.float32)
+    token_count, width = residual.shape
+    chips = lax.axis_size("tp") // 2
+    projected = tp_sum(
+        jnp.dot(rows_here, out_weight, preferred_element_type=jnp.float32)
+        .astype(jnp.bfloat16)
+        .reshape(chips, 2, token_count, width)
+    )
     stream = residual.astype(jnp.float32) + projected
     mean_value = stream.mean(-1, keepdims=True)
     centred = stream - mean_value
     variance = (centred * centred).mean(-1, keepdims=True)
     normed = (centred * lax.rsqrt(variance + layer_epsilon) * norm_gain).astype(jnp.bfloat16)
-    token_count = residual.shape[0]
-    width = residual.shape[1]
+    spans = lax.axis_size("sp")
     route_count = routes.shape[1]
-    expert_count = lax.axis_size("sp") * gate_weight.shape[0]
-    capacity = 9 * route_count * token_count // (8 * expert_count)
+    capacity = 9 * route_count * token_count // (8 * spans)
+    slots = -(-capacity // 8) * 8
     flat_routes = routes.reshape(-1)
-    one_hot = (flat_routes[:, None] == jnp.arange(expert_count)[None, :]).astype(jnp.int32)
+    one_hot = (flat_routes[:, None] == jnp.arange(spans)[None, :]).astype(jnp.int32)
     slot_ids = jnp.sum((jnp.cumsum(one_hot, axis=0) - 1) * one_hot, axis=1)
-    destination = flat_routes * capacity + slot_ids
-    slot_range = jnp.arange(expert_count * capacity)
-    selector = jnp.any(
-        slot_range[:, None, None] == destination.reshape(token_count, route_count)[None], axis=2
-    )
-    dispatch = jnp.dot(
-        selector.astype(jnp.bfloat16), normed, preferred_element_type=jnp.float32
-    ).astype(jnp.bfloat16)
-    inbound = lax.all_to_all(
-        dispatch.reshape(expert_count, capacity, width),
-        "sp",
-        split_axis=0,
-        concat_axis=0,
-        tiled=True,
-    )
-    arrived = inbound.reshape(-1, width)
-    row_piece = lax.all_gather(arrived, "tp", axis=0, tiled=True)
-    gate = jnp.dot(row_piece, gate_weight[0], preferred_element_type=jnp.float32)
-    upward = jnp.dot(row_piece, up_weight[0], preferred_element_type=jnp.float32)
+    destination = (flat_routes * slots + slot_ids).astype(jnp.float32)
+    notes = jnp.concatenate(
+        [destination.reshape(token_count, route_count).T, route_weights.T], axis=0
+    )
+    notes = jnp.pad(
+        notes,
+        ((0, -2 * route_count % 8), (0, -token_count % 128)),
+        constant_values=-1.0,
+    )
+    arrived, all_notes = spread(normed, notes, chips, spans, slots, route_count)
+    rows_in = arrived.reshape(-1, width)
+    gate = jnp.dot(rows_in, gate_weight[0], preferred_element_type=jnp.float32)
+    upward = jnp.dot(rows_in, up_weight[0], preferred_element_type=jnp.float32)
     hidden = (jax.nn.silu(gate) * upward).astype(jnp.bfloat16)
-    rows_here = hidden
-    partial_value = jnp.dot(rows_here, down_weight[0], preferred_element_type=jnp.float32).astype(
+    partial_value = jnp.dot(hidden, down_weight[0], preferred_element_type=jnp.float32).astype(
         jnp.bfloat16
     )
-    returned = lax.psum_scatter(
-        lax.optimization_barrier(partial_value).astype(jnp.float32).astype(jnp.bfloat16),
-        "tp",
-        scatter_dimension=0,
-        tiled=True,
-    )
-    back_rows = lax.all_to_all(
-        returned.reshape(inbound.shape), "sp", split_axis=0, concat_axis=0, tiled=True
-    ).reshape(-1, width)
-    picked = back_rows[destination].astype(jnp.float32).reshape(token_count, route_count, width)
-    combined = jnp.sum(picked * route_weights[..., None], axis=1)
+    places = all_notes[:, None, :route_count, :token_count, None]
+    weights = all_notes[:, None, route_count : 2 * route_count, :token_count, None]
+    slot_range = jnp.arange(spans * slots).astype(jnp.float32).reshape(1, spans, 1, 1, slots)
+    shares = jnp.sum(jnp.where(places == slot_range, weights, 0.0), axis=2).astype(jnp.bfloat16)
+    combined = collect(partial_value.reshape(arrived.shape), shares)
     return (stream + combined).astype(jnp.bfloat16)
 
 

time: 233 us -> 185 us (0.79)
  waiting for transfers between devices: 147 us -> 0.01 us
  Pallas kernels: 0 us -> 127 us
  between operations: 13.4 us -> 0.21 us
  blocking collectives: 11.9 us -> 0 us
  local copies, waits for them, and re-layouts: 9.97 us -> 5.02 us
  starting transfers between devices: 11 us -> 6.78 us
  other arithmetic: 9.64 us -> 13.3 us
  matrix products: 28.7 us -> 32.3 us
    pallas_call x0 -> x3, Pallas kernels: none -> 127 us  [the longest x1 54 us: collect(): pl.pallas_call(functools.partial(collect_kernel, chips, spans), out_shape...]
    reduce_scatter x2 -> x0, waiting for transfers between devices: 85.1 us -> none  [the longest x1 52.2 us: local(): lax.psum_scatter(lax.optimization_barrier(partial_value).astype(jnp.float...]
    all_gather x1 -> x0, waiting for transfers between devices: 51.3 us -> none  [local(): row_piece = lax.all_gather(arrived, 'tp', axis=0, tiled=True)]
    all_to_all x1 -> x0, blocking collectives: 11.9 us -> none  [local(): lax.all_to_all(dispatch.reshape(expert_count, capacity, width), 'sp', spl...]
    all_to_all x1 -> x0, waiting for transfers between devices: 10.4 us -> none  [local(): lax.all_to_all(returned.reshape(inbound.shape), 'sp', split_axis=0, conca...]
    dot_general x4 -> x2, matrix products: 21.5 us -> 27.5 us  [the longest x1 17.6 us: local(): jnp.dot(hidden, down_weight[0], preferred_element_type=jnp.float32)]
    all_to_all x1 -> x0, starting transfers between devices: 3.9 us -> none  [local(): lax.all_to_all(returned.reshape(inbound.shape), 'sp', split_axis=0, conca...]
    reshape x4 -> x0, local copies, waits for them, and re-layouts: 3.2 us -> none  [the longest x1 2.01 us: local(): returned.reshape(inbound.shape)]
  transfers between devices with their start and end apart: 6 -> 2, of which waited for: 4 -> 0; matrix products, arithmetic and copies ran while one was open for 2% -> 4% of each run, Pallas kernels for 0% -> 0%
where the time goes in v1:
time: 185 us
  Pallas kernels  127 us (69%)
  matrix products  32.3 us (17%)
  other arithmetic  13.3 us (7%)
  starting transfers between devices  6.78 us (4%)
  local copies, waits for them, and re-layouts  5.02 us (3%)
    pallas_call x1, Pallas kernels, collect(): pl.pallas_call(functools.partial(collect_kernel, chips, spans), out_shape...  54 us
    pallas_call x1, Pallas kernels, spread(): pl.pallas_call(functools.partial(spread_kernel, chips, spans, picks), out...  40.5 us
    pallas_call x1, Pallas kernels, tp_sum(): pl.pallas_call(functools.partial(sum_kernel, chips), out_shape=jax.ShapeD...  32.7 us
    dot_general x1, matrix products, local(): jnp.dot(hidden, down_weight[0], preferred_element_type=jnp.float32)  17.6 us
    dot_general x1, matrix products, local(): gate = jnp.dot(rows_in, gate_weight[0], preferred_element_type=jnp.float32)  9.98 us
    ppermute x2, starting transfers between devices, passed_along(): lax.ppermute(value, axis, [(source, source + steps) for source in range(f...  6.78 us
  transfers between devices with their start and end apart: 2, of which 0 were waited for; matrix products, arithmetic and copies ran while one was open for 4% of the time, Pallas kernels for 0%

profile of v1, /device:TPU:8, one launch (start us, length us, event | category | flops | bytes accessed | tf_op | source)
XLA Modules:
  0.0 184.8 jit_solution(4665433414625580945)
XLA Ops:
  0.0 0.9 pad_maximum_fusion.2
  0.9 3.4 %collective-permute-start = (bf16[127,256]{1,0:T(8,128)(2,1)S(1)}, bf16[127,256]{1,0:T(8,128)(2,1)S(1)}, u32[]{:S(2)}, u32[]{:S(2)}) collective-permute-start(bf16[127,256]{1,0:T(8,128)(2,1)S(1)} %pad_maximum_fusion.2), channel_id=1, source_target_pairs={{0,8},{8,16},{16,24},{1,9},{9,17},{17,25},{2,10},{10,18},{18,26},{... | collective-permute-start | bytes 195080 | tf_op jit(solution)/shard_map/ppermute | solution.py:22
  5.1 3.4 %collective-permute-start.1 = (bf16[127]{0:T(256)(128)(2,1)S(1)}, bf16[127]{0:T(256)(128)(2,1)S(1)}, u32[]{:S(2)}, u32[]{:S(2)}) collective-permute-start(bf16[127]{0:T(256)(128)(2,1)S(1)} %slice.24), channel_id=1, source_target_pairs={{0,8},{8,16},{16,24},{1,9},{9,17},{17,25},{2,10},{10,18},{18,26},{... | collective-permute-start | bytes 770 | tf_op jit(solution)/shard_map/ppermute | solution.py:22
  8.5 0.8 copy.37
  10.0 0.7 convert_bitcast_fusion
  10.7 1.3 select_maximum_fusion.notes
  12.0 1.1 copy.35
  13.1 0.7 max.16
  14.4 1.0 pad_maximum_fusion
  15.8 1.1 fusion.2
  17.0 1.2 fusion
  18.2 1.6 fusion.20
  19.9 2.1 %convolution_convert_fusion.1 = bf16[512,2048]{1,0:T(8,128)(2,1)} fusion(bf16[512,256]{0,1:T(8,128)(2,1)S(1)} %bitcast.68, bf16[256,2048]{1,0:T(8,128)(2,1)S(1)} %copy-done), kind=kOutput, calls=%fused_computation.11 | convolution fusion | flops 537919488 | bytes 3407872 | tf_op jit(solution)/shard_map/dot_general | solution.py:544
  22.0 32.7 %shard_map.127 = f32[64,2048]{1,0:T(8,128)} custom-call(bf16[4,2,64,2048]{3,2,1,0:T(8,128)(2,1)} %bitcast.66), custom_call_target="tpu_custom_call" | custom-call | tf_op jit(solution)/shard_map/pallas_call | solution.py:182
  54.7 1.2 fusion.24
  55.9 1.3 multiply_reduce_fusion
  57.2 1.9 %multiply_convert_fusion.1.normed = bf16[64,2048]{1,0:T(8,128)(2,1)} fusion(f32[2048]{0:T(1024)S(1)} %copy-done.3, f32[64]{0:T(128)S(1)} %add_rsqrt_fusion, f32[64]{0:T(128)S(1)} %broadcast_multiply_fusion, f32[64,2048]{1,0:T(8,128)} %shard_map.127, bf16[64,2048]{1,0:T(8,128)(2,1)S(1)} %copy-done.2), kind=kLoop, calls=%fused_computation.24 | loop fusion | flops 786432 | bytes 1057280 | tf_op jit(solution)/shard_map/convert_element_type | solution.py:552
  59.1 40.5 %shard_map.128 = (bf16[2,4,4,40,2048]{4,3,2,1,0:T(8,128)(2,1)}, f32[4,8,128]{2,1,0:T(8,128)}) custom-call(bf16[64,2048]{1,0:T(8,128)(2,1)} %multiply_convert_fusion.1.normed, f32[8,128]{1,0:T(8,128)} %select_maximum_fusion.notes), custom_call_target="tpu_custom_call" | custom-call | tf_op jit(solution)/shard_map/pallas_call | solution.py:332
  99.6 0.8 fusion.29
  100.6 0.9 copy.39.shares
  101.4 10.0 %fusion.5 = f32[1280,896]{1,0:T(8,128)} fusion(bf16[1280,2048]{1,0:T(8,128)(2,1)} %bitcast.73, bf16[1,2048,896]{2,1,0:T(8,128)(2,1)} %param.23), kind=kOutput, calls=%fused_computation.9 | convolution fusion | flops 4697620480 | bytes 13500416 | tf_op jit(solution)/shard_map/dot_general | solution.py:571
  111.4 17.6 %convolution_convert_fusion = bf16[1280,2048]{1,0:T(8,128)(2,1)} fusion(bf16[1,896,2048]{2,1,0:T(8,128)(2,1)} %param.25, f32[1280,896]{1,0:T(8,128)} %fusion.5, bf16[1280,2048]{1,0:T(8,128)(2,1)} %bitcast.74, bf16[1,2048,896]{2,1,0:T(8,128)(2,1)} %param.24), kind=kOutput, calls=%fused_computation | convolution fusion | flops 9404743680 | bytes 22413312 | tf_op jit(solution)/shard_map/dot_general | solution.py:574
  129.0 54.0 %shard_map.129 = f32[64,2048]{1,0:T(8,128)} custom-call(bf16[2,4,4,40,2048]{4,3,2,1,0:T(8,128)(2,1)} %bitcast.67, bf16[4,4,64,40]{3,2,1,0:T(8,128)(2,1)} %copy.39.shares), custom_call_target="tpu_custom_call" | custom-call | tf_op jit(solution)/shard_map/pallas_call | solution.py:442
  183.0 1.9 %add_convert_fusion = bf16[64,2048]{1,0:T(8,128)(2,1)} fusion(f32[64,2048]{1,0:T(8,128)} %shard_map.129, f32[64,2048]{1,0:T(8,128)S(1)} %copy-done.1, bf16[64,2048]{1,0:T(8,128)(2,1)S(1)} %copy-done.2), kind=kLoop, calls=%fused_computation.23 | loop fusion | flops 524288 | bytes 1572864 | tf_op jit(solution)/shard_map/convert_element_type | solution.py:582
  (31 shorter events, 2.8 us)
Async XLA Ops:
  0.0 19.9 %copy-start = (bf16[256,2048]{1,0:T(8,128)(2,1)S(1)}, bf16[256,2048]{1,0:T(8,128)(2,1)}, u32[]{:S(2)}) copy-start(bf16[256,2048]{1,0:T(8,128)(2,1)} %param.18) | copy-start | bytes 3145732
  0.9 13.5 %collective-permute-start = (bf16[127,256]{1,0:T(8,128)(2,1)S(1)}, bf16[127,256]{1,0:T(8,128)(2,1)S(1)}, u32[]{:S(2)}, u32[]{:S(2)}) collective-permute-start(bf16[127,256]{1,0:T(8,128)(2,1)S(1)} %pad_maximum_fusion.2), channel_id=1, source_target_pairs={{0,8},{8,16},{16,24},{1,9},{9,17},{17,25},{2,10},{10,18},{18,26},{... | collective-permute-start | bytes 195080 | tf_op jit(solution)/shard_map/ppermute | solution.py:22
  5.1 8.8 %collective-permute-start.1 = (bf16[127]{0:T(256)(128)(2,1)S(1)}, bf16[127]{0:T(256)(128)(2,1)S(1)}, u32[]{:S(2)}, u32[]{:S(2)}) collective-permute-start(bf16[127]{0:T(256)(128)(2,1)S(1)} %slice.24), channel_id=1, source_target_pairs={{0,8},{8,16},{16,24},{1,9},{9,17},{17,25},{2,10},{10,18},{18,26},{... | collective-permute-start | bytes 770 | tf_op jit(solution)/shard_map/ppermute | solution.py:22
  19.8 34.9 %copy-start.2 = (bf16[64,2048]{1,0:T(8,128)(2,1)S(1)}, bf16[64,2048]{1,0:T(8,128)(2,1)}, u32[]{:S(2)}) copy-start(bf16[64,2048]{1,0:T(8,128)(2,1)} %param.19) | copy-start | bytes 786436
  19.8 37.4 %copy-start.3 = (f32[2048]{0:T(1024)S(1)}, f32[2048]{0:T(1024)}, u32[]{:S(2)}) copy-start(f32[2048]{0:T(1024)} %param.20) | copy-start | bytes 24580
  128.9 54.0 %copy-start.1 = (f32[64,2048]{1,0:T(8,128)S(1)}, f32[64,2048]{1,0:T(8,128)}, u32[]{:S(2)}) copy-start(f32[64,2048]{1,0:T(8,128)} %shard_map.127) | copy-start | bytes 1572868

commit v2 on v1

--- a/solution.py
+++ b/solution.py
@@ -61,11 +61,14 @@
     pl.semaphore_wait(barrier, inner + spans)
 
 
-def outside_in(count):
-    order = []
-    for step in range((count + 1) // 2):
-        order.extend([count - 1 - step] + ([step] if step != count - 1 - step else []))
-    return order
+def line_order(chips, visit):
+    chip = tp_place()[0]
+    for time in range(chips - 1):
+        onward = chips - 1 - (time - chip)
+        back = time - (chips - 1 - chip)
+        pl.when((time >= chip) & (onward > chip))(lambda onward=onward: visit(onward, 0))
+        pl.when((back >= 0) & (back < chip))(lambda back=back: visit(back, 1))
+    visit(chip, None)
 
 
 def column_loop(width, body):
@@ -78,42 +81,40 @@
     lax.fori_loop(0, width // step, one, 0)
 
 
-def line_step(chips, block, term, width, total, travel, held, sent, landed):
+def line_step(chips, block, way, term, width, total, travel, held, sent, landed):
     chip, _, _, before, after = tp_place()
-    for way, passes, receives, device in (
-        (0, chip < block, chip > 0, {"tp": after}),
-        (1, chip > block, chip < chips - 1, {"tp": before}),
-    ):
-        copy = remote(
-            travel.at[block], held.at[way, block], sent.at[block], landed.at[way, block], device
-        )
-
-        @pl.when(passes & receives)
-        def _(copy=copy, way=way):
-            copy.wait_recv()
-
-            def add(columns):
-                travel[block, :, columns] = (
-                    term(columns) + held[way, block, :, columns].astype(jnp.float32)
-                ).astype(jnp.bfloat16)
-
-            column_loop(width, add)
-
-        @pl.when(passes & jnp.logical_not(receives))
-        def _():
-            def keep(columns):
-                travel[block, :, columns] = term(columns).astype(jnp.bfloat16)
-
-            column_loop(width, keep)
-
-        pl.when(passes)(copy.start)
-
-    @pl.when(chip == block)
+    if way is None:
+
+        def own(columns):
+            total[:, columns] = term(columns)
+
+        column_loop(width, own)
+        return
+    receives = chip > 0 if way == 0 else chip < chips - 1
+    device = {"tp": after if way == 0 else before}
+    copy = remote(
+        travel.at[block], held.at[way, block], sent.at[block], landed.at[way, block], device
+    )
+
+    @pl.when(receives)
+    def _():
+        copy.wait_recv()
+
+        def add(columns):
+            travel[block, :, columns] = (
+                term(columns) + held[way, block, :, columns].astype(jnp.float32)
+            ).astype(jnp.bfloat16)
+
+        column_loop(width, add)
+
+    @pl.when(jnp.logical_not(receives))
     def _():
         def keep(columns):
-            total[:, columns] = term(columns)
+            travel[block, :, columns] = term(columns).astype(jnp.bfloat16)
 
         column_loop(width, keep)
+
+    copy.start()
 
 
 def line_finish(chips, width, total, travel, held, sent, landed):
@@ -160,17 +161,19 @@
             {"tp": partner},
         )
 
-    for block in outside_in(chips):
-        handed(block).start()
-    for block in outside_in(chips):
+    line_order(chips, lambda block, way: handed(block).start())
+
+    def visit(block, way):
         handed(block).wait_recv()
 
-        def term(columns, block=block):
+        def term(columns):
             return parts[block, core, :, columns].astype(jnp.float32) + arrived[
                 block, :, columns
             ].astype(jnp.float32)
 
-        line_step(chips, block, term, width, total, travel, held, sent, landed)
+        line_step(chips, block, way, term, width, total, travel, held, sent, landed)
+
+    line_order(chips, visit)
     line_finish(chips, width, total, travel, held, sent, landed)
     for block in range(chips):
         handed(block).wait_send()
@@ -194,7 +197,7 @@
             dma((2, chips)),
         ],
         compiler_params=pltpu.CompilerParams(
-            collective_id=0, has_side_effects=True, vmem_limit_bytes=60 << 20
+            collective_id=0, has_side_effects=True, vmem_limit_bytes=min(60 << 20, 8 * parts.size + (6 << 20))
         ),
     )(parts)
 
@@ -265,21 +268,20 @@
 
     def hand_out(block, source, note):
         listing = note[...][:picks, :count]
-        for expert in range(spans):
-            slot = (
-                lax.broadcasted_iota(jnp.int32, (slots, count), 0) + expert * slots
-            ).astype(jnp.float32)
-            chosen = jnp.zeros((slots, count), jnp.float32)
-            for pick in range(picks):
-                chosen = jnp.where(slot == listing[pick : pick + 1], 1.0, chosen)
-            chosen = chosen.astype(jnp.bfloat16)
-
-            def select(columns, expert=expert, chosen=chosen):
-                outgoing[block, expert, :, columns] = jnp.dot(
-                    chosen, source[:, columns], preferred_element_type=jnp.float32
-                ).astype(jnp.bfloat16)
-
-            column_loop(width, select)
+        slot = lax.broadcasted_iota(jnp.int32, (spans * slots, count), 0).astype(jnp.float32)
+        chosen = jnp.zeros((spans * slots, count), jnp.float32)
+        for pick in range(picks):
+            chosen = jnp.where(slot == listing[pick : pick + 1], 1.0, chosen)
+        chosen = chosen.astype(jnp.bfloat16)
+
+        def select(columns):
+            picked = jnp.dot(chosen, source[:, columns], preferred_element_type=jnp.float32)
+            for expert in range(spans):
+                outgoing[block, expert, :, columns] = picked[
+                    expert * slots : (expert + 1) * slots
+                ].astype(jnp.bfloat16)
+
+        column_loop(width, select)
         for step in range(1, spans):
             to_span(block, step).start()
         rows[core, block, span] = outgoing[block, span]
@@ -350,7 +352,7 @@
             dma((chips,)),
         ],
         compiler_params=pltpu.CompilerParams(
-            collective_id=1, has_side_effects=True, vmem_limit_bytes=60 << 20
+            collective_id=1, has_side_effects=True, vmem_limit_bytes=min(60 << 20, 8 * chips * spans * slots * width + (8 << 20))
         ),
     )(normed, notes)
 
@@ -397,12 +399,12 @@
             {"sp": other},
         )
 
-    for block in outside_in(chips):
-        handed(block).start()
-    for block in outside_in(chips):
+    line_order(chips, lambda block, way: handed(block).start())
+
+    def send_out(block, way):
         handed(block).wait_recv()
 
-        def add(columns, block=block):
+        def add(columns):
             outgoing[block, :, :, columns] = (
                 parts[core, block, :, :, columns].astype(jnp.float32)
                 + arrived[block, :, :, columns].astype(jnp.float32)
@@ -412,11 +414,14 @@
         for step in range(1, spans):
             to_span(block, step).start()
         gathered[block, span] = outgoing[block, span]
-    for block in outside_in(chips):
+
+    line_order(chips, send_out)
+
+    def visit(block, way):
         for step in range(1, spans):
             to_span(block, step).wait_recv()
 
-        def term(columns, block=block):
+        def term(columns):
             result = None
             for expert in range(spans):
                 share = jnp.dot(
@@ -427,7 +432,9 @@
                 result = share if result is None else result + share
             return result
 
-        line_step(chips, block, term, width, total, travel, held, sent, landed)
+        line_step(chips, block, way, term, width, total, travel, held, sent, landed)
+
+    line_order(chips, visit)
     line_finish(chips, width, total, travel, held, sent, landed)
     for block in range(chips):
         handed(block).wait_send()
@@ -458,7 +465,7 @@
             dma((2, chips)),
         ],
         compiler_params=pltpu.CompilerParams(
-            collective_id=2, has_side_effects=True, vmem_limit_bytes=60 << 20
+            collective_id=2, has_side_effects=True, vmem_limit_bytes=min(60 << 20, 6 * parts.size + (8 << 20))
         ),
     )(parts, shares)
 
@@ -486,18 +493,21 @@
     reach_back = WINDOW - 1
     score_scale = 1.0 / math.sqrt(HEAD_DIM)
     doc_float = (doc_ids + 1).astype(jnp.float32)
-    key_value = jnp.concatenate([keys, values], axis=1).astype(jnp.float32)
-    tail_pairs, tail_docs = (
-        passed_along(key_value[span_rows - reach_back :].astype(jnp.bfloat16), "sp", 1).astype(
-            jnp.float32
+    tails = passed_along(
+        jnp.concatenate(
+            [
+                keys[span_rows - reach_back :],
+                values[span_rows - reach_back :],
+                doc_float[span_rows - reach_back :, None].astype(jnp.bfloat16),
+            ],
+            axis=1,
         ),
-        passed_along(doc_float[span_rows - reach_back :].astype(jnp.bfloat16), "sp", 1).astype(
-            jnp.float32
-        ),
-    )
-    all_keys = jnp.concatenate([tail_pairs[:, :kv_width].astype(jnp.bfloat16), keys], axis=0)
-    all_values = jnp.concatenate([tail_pairs[:, kv_width:].astype(jnp.bfloat16), values], axis=0)
-    all_docs = jnp.concatenate([tail_docs, doc_float], axis=0)
+        "sp",
+        1,
+    )
+    all_keys = jnp.concatenate([tails[:, :kv_width], keys], axis=0)
+    all_values = jnp.concatenate([tails[:, kv_width : 2 * kv_width], values], axis=0)
+    all_docs = jnp.concatenate([tails[:, 2 * kv_width].astype(jnp.float32), doc_float], axis=0)
     block_rows = min(512, span_rows)
     sink_table = sink_logits.reshape(kv_groups, group_ratio, 1)
     offsets = (

time: 185 us -> 151 us (0.82); the launches traced: 185 us -> 148 us
  Pallas kernels: 127 us -> 96.5 us
  other arithmetic: 13.3 us -> 7.07 us
  local copies, waits for them, and re-layouts: 5.02 us -> 10 us
  starting transfers between devices: 6.78 us -> 3.4 us
    pallas_call x1, Pallas kernels: 54 us -> 36 us  [collect(): pl.pallas_call(functools.partial(collect_kernel, chips, spans), out_shape...]
    pallas_call x1, Pallas kernels: 32.7 us -> 25.5 us  [tp_sum(): pl.pallas_call(functools.partial(sum_kernel, chips), out_shape=jax.ShapeD...]
    pallas_call x1, Pallas kernels: 40.5 us -> 35 us  [spread(): pl.pallas_call(functools.partial(spread_kernel, chips, spans, picks), out...]
    unnamed x10 -> x12, local copies, waits for them, and re-layouts: 1.88 us -> 6.66 us
    ppermute x2 -> x1, starting transfers between devices: 6.78 us -> 3.4 us  [passed_along(): lax.ppermute(value, axis, [(source, source + steps) for source in range(f...]
  transfers between devices with their start and end apart: 2 -> 1, of which waited for: 0 -> 0; matrix products, arithmetic and copies ran while one was open for 4% -> 3% of each run, Pallas kernels for 0% -> 0%
where the time goes in v2:
time: 151 us; the launch traced here: 148 us
  Pallas kernels  96.5 us (64%)
  matrix products  30.9 us (20%)
  local copies, waits for them, and re-layouts  10 us (7%)
  other arithmetic  7.07 us (5%)
  starting transfers between devices  3.4 us (2%)
    pallas_call x1, Pallas kernels, collect(): pl.pallas_call(functools.partial(collect_kernel, chips, spans), out_shape...  36 us
    pallas_call x1, Pallas kernels, spread(): pl.pallas_call(functools.partial(spread_kernel, chips, spans, picks), out...  35 us
    pallas_call x1, Pallas kernels, tp_sum(): pl.pallas_call(functools.partial(sum_kernel, chips), out_shape=jax.ShapeD...  25.5 us
    dot_general x1, matrix products, local(): jnp.dot(hidden, down_weight[0], preferred_element_type=jnp.float32)  17.6 us
    dot_general x1, matrix products, local(): gate = jnp.dot(rows_in, gate_weight[0], preferred_element_type=jnp.float32)  9.99 us
    unnamed x12, local copies, waits for them, and re-layouts  6.66 us
    ppermute x1, starting transfers between devices, passed_along(): lax.ppermute(value, axis, [(source, source + steps) for source in range(f...  3.4 us
  transfers between devices with their start and end apart: 1, of which 0 were waited for; matrix products, arithmetic and copies ran while one was open for 3% of the time, Pallas kernels for 0%

profile of v2, /device:TPU:8, one launch (start us, length us, event | category | flops | bytes accessed | tf_op | source)
XLA Modules:
  0.0 148.0 jit_solution(12842110597040989623)
XLA Ops:
  0.0 0.8 add_convert_fusion.2
  1.0 0.8 slice.26
  1.8 0.8 slice.25
  2.6 3.4 %collective-permute-start = (bf16[127,257]{1,0:T(8,128)(2,1)S(1)}, bf16[127,257]{1,0:T(8,128)(2,1)S(1)}, u32[]{:S(2)}, u32[]{:S(2)}) collective-permute-start(bf16[127,257]{1,0:T(8,128)(2,1)S(1)} %pad_maximum_fusion.2), channel_id=1, source_target_pairs={{0,8},{8,16},{16,24},{1,9},{9,17},{17,25},{2,10},{10,18},{18,26},{... | collective-permute-start | bytes 195842 | tf_op jit(solution)/shard_map/ppermute | solution.py:22
  6.0 1.1 copy.39
  7.1 0.7 max.16
  7.8 0.8 copy.41
  9.4 0.7 convert_bitcast_fusion
  10.1 0.7 select_maximum_fusion.notes
  10.8 1.0 pad_maximum_fusion
  12.4 0.5 fusion.13
  12.9 1.1 fusion.2
  14.0 1.1 fusion
  15.2 1.5 %fusion.20 = bf16[512,2,2,64]{0,3,2,1:T(8,128)(2,1)S(1)} fusion(bf16[639,2,64,1]{0,2,3,1:T(8,128)(2,1)S(1)} %bitcast.74, f32[2,639,512,2]{2,1,3,0:T(8,128)S(1)} %get-tuple-element.16, f32[2,2,512]{2,1,0:T(2,128)S(1)} %broadcast_maximum_fusion, pred[512,639]{0,1:T(8,128)(4,1)S(1)} %fusion.13, f32[512,2,2]{0,2,1:T(2,128)S(1)} %add_bitcast_fusion), kind=kOutput, calls=%fused_computation.21 | convolution fusion | flops 173006848 | bytes 6003968 | tf_op jit(solution)/shard_map/grbs,sgd->bgrd/dot_general | solution.py:541
  16.8 0.7 convolution_convert_fusion.1
  17.5 25.5 %shard_map.127 = f32[64,2048]{1,0:T(8,128)S(1)} custom-call(bf16[4,2,64,2048]{3,2,1,0:T(8,128)(2,1)S(1)} %bitcast.68), custom_call_target="tpu_custom_call" | custom-call | tf_op jit(solution)/shard_map/pallas_call | solution.py:185
  43.2 0.2 multiply_reduce_fusion
  43.5 35.0 %shard_map.128 = (bf16[2,4,4,40,2048]{4,3,2,1,0:T(8,128)(2,1)S(1)}, f32[4,8,128]{2,1,0:T(8,128)S(1)}) custom-call(bf16[64,2048]{1,0:T(8,128)(2,1)S(1)} %multiply_convert_fusion.1.normed, f32[8,128]{1,0:T(8,128)S(1)} %select_maximum_fusion.notes), custom_call_target="tpu_custom_call" | custom-call | tf_op jit(solution)/shard_map/pallas_call | solution.py:334
  78.6 2.3 %copy-done.2 = bf16[2,4,4,40,2048]{4,3,2,1,0:T(8,128)(2,1)} copy-done((bf16[2,4,4,40,2048]{4,3,2,1,0:T(8,128)(2,1)}, bf16[2,4,4,40,2048]{4,3,2,1,0:T(8,128)(2,1)S(1)}, u32[]{:S(2)}) %copy-start.2) | copy-done | bytes 5242904
  81.2 10.0 %fusion.5 = f32[1280,896]{1,0:T(8,128)} fusion(bf16[1280,2048]{1,0:T(8,128)(2,1)} %bitcast.70, bf16[1,2048,896]{2,1,0:T(8,128)(2,1)} %param.23), kind=kOutput, calls=%fused_computation.9 | convolution fusion | flops 4697620480 | bytes 13500416 | tf_op jit(solution)/shard_map/dot_general | solution.py:581
  91.2 17.6 %convolution_convert_fusion = bf16[1280,2048]{1,0:T(8,128)(2,1)} fusion(bf16[1,896,2048]{2,1,0:T(8,128)(2,1)} %param.25, f32[1280,896]{1,0:T(8,128)} %fusion.5, bf16[1280,2048]{1,0:T(8,128)(2,1)} %bitcast.71, bf16[1,2048,896]{2,1,0:T(8,128)(2,1)} %param.24), kind=kOutput, calls=%fused_computation | convolution fusion | flops 9404743680 | bytes 22413312 | tf_op jit(solution)/shard_map/dot_general | solution.py:584
  108.8 2.5 %copy-done.1 = bf16[1280,2048]{1,0:T(8,128)(2,1)S(1)} copy-done((bf16[1280,2048]{1,0:T(8,128)(2,1)S(1)}, bf16[1280,2048]{1,0:T(8,128)(2,1)}, u32[]{:S(2)}) %copy-start.1) | copy-done | bytes 5242904
  111.3 36.0 %shard_map.129 = f32[64,2048]{1,0:T(8,128)S(1)} custom-call(bf16[2,4,4,40,2048]{4,3,2,1,0:T(8,128)(2,1)S(1)} %bitcast.69, bf16[4,4,64,40]{3,2,1,0:T(8,128)(2,1)S(1)} %copy.43.shares), custom_call_target="tpu_custom_call" | custom-call | tf_op jit(solution)/shard_map/pallas_call | solution.py:449
  147.2 0.8 add_convert_fusion
  (34 shorter events, 2.4 us)
Async XLA Ops:
  0.0 16.8 %copy-start = (bf16[256,2048]{1,0:T(8,128)(2,1)S(1)}, bf16[256,2048]{1,0:T(8,128)(2,1)}, u32[]{:S(2)}) copy-start(bf16[256,2048]{1,0:T(8,128)(2,1)} %param.18) | copy-start | bytes 3145732
  2.6 8.2 %collective-permute-start = (bf16[127,257]{1,0:T(8,128)(2,1)S(1)}, bf16[127,257]{1,0:T(8,128)(2,1)S(1)}, u32[]{:S(2)}, u32[]{:S(2)}) collective-permute-start(bf16[127,257]{1,0:T(8,128)(2,1)S(1)} %pad_maximum_fusion.2), channel_id=1, source_target_pairs={{0,8},{8,16},{16,24},{1,9},{9,17},{17,25},{2,10},{10,18},{18,26},{... | collective-permute-start | bytes 195842 | tf_op jit(solution)/shard_map/ppermute | solution.py:22
  16.7 26.2 %copy-start.3 = (bf16[64,2048]{1,0:T(8,128)(2,1)S(1)}, bf16[64,2048]{1,0:T(8,128)(2,1)}, u32[]{:S(2)}) copy-start(bf16[64,2048]{1,0:T(8,128)(2,1)} %param.19) | copy-start | bytes 786436
  16.8 26.6 %copy-start.4 = (f32[2048]{0:T(1024)S(1)}, f32[2048]{0:T(1024)}, u32[]{:S(2)}) copy-start(f32[2048]{0:T(1024)} %param.20) | copy-start | bytes 24580
  78.6 2.3 %copy-start.2 = (bf16[2,4,4,40,2048]{4,3,2,1,0:T(8,128)(2,1)}, bf16[2,4,4,40,2048]{4,3,2,1,0:T(8,128)(2,1)S(1)}, u32[]{:S(2)}) copy-start(bf16[2,4,4,40,2048]{4,3,2,1,0:T(8,128)(2,1)S(1)} %get-tuple-element.7) | copy-start | bytes 15728644
  108.8 2.5 %copy-start.1 = (bf16[1280,2048]{1,0:T(8,128)(2,1)S(1)}, bf16[1280,2048]{1,0:T(8,128)(2,1)}, u32[]{:S(2)}) copy-start(bf16[1280,2048]{1,0:T(8,128)(2,1)} %convolution_convert_fusion) | copy-start | bytes 15728644
